TPU v7x, 512 devices: a whole 4x8x8 slice. The times are simulated.
512 devices in a mesh: sp: 32 (over z, x), tp: 16 (over y, core).
Axes of the slice: x: 4, y: 8, z: 8, core: 2. Of those that a mesh axis runs over, the one named last changes fastest.
Arguments:
- queries: bfloat16 [8192, 1024], P('sp', 'tp'), may hold values from -6 to 6
- keys: bfloat16 [8192, 256], P('sp'), may hold values from -6 to 6
- values: bfloat16 [8192, 256], P('sp'), may hold values from -6 to 6
- sink: float32 [16], P('tp'), may hold values from 3 to 6
- w_out: bfloat16 [1024, 2048], P('tp'), may hold values from -0.1875 to 0.1875
- stream: bfloat16 [8192, 2048], P(('sp', 'tp')), may hold values from -6 to 6
- gain: bfloat16 [2048], replicated, may hold values from 0.099609375 to 1.8984375
- routes: int32 [8192, 4], P('sp'), may hold values from 0 to 63, all different within a row; in each aligned block of 16 rows (0 to 15, 16 to 31, ...) at most 2 rows name the same one
- route_weights: float32 [8192, 4], P('sp'), may hold values from 0.2 to 1
- w_gate: bfloat16 [64, 1024, 2048], P('sp', 'tp'), may hold values from -0.125 to 0.125
- w_up: bfloat16 [64, 1024, 2048], P('sp', 'tp'), may hold values from -0.125 to 0.125
- w_down: bfloat16 [64, 1024, 2048], P('sp', None, 'tp'), may hold values from -0.1875 to 0.1875
- shared_gate: bfloat16 [1024, 2048], P('tp'), may hold values from -0.125 to 0.125
- shared_up: bfloat16 [1024, 2048], P('tp'), may hold values from -0.125 to 0.125
- shared_down: bfloat16 [1024, 2048], P(None, 'tp'), may hold values from -0.1875 to 0.1875
Outputs:
- layer_out: bfloat16 [8192, 2048], P('sp', 'tp')
Inputs may be any that keep to these rules, and one draw needn't show every extreme that they name: `routes`: in each aligned block of 16 rows no expert is named in more than 2 rows, and some blocks reach 2; a row names 4 different experts.
All inputs are finite; a program needn't handle non-finite values.
Results may differ from a plain program's by a relative error of at most 0.014.
Values may be sent and summed in bfloat16 or wider, within the bound.
A program may use at most 64 MiB of HBM per device.

v0:
```python
import jax
import jax.numpy as jnp
from jax import lax
from jax.sharding import PartitionSpec as P

D = 2048
HEADS = 16
KV_HEADS = 4
HD = 64
WINDOW = 128
EXPERTS = 64
TOPK = 4


NORM_EPS = 1e-05


def with_halo(array, sides, width):
    for axis, dim in sides:
        devices, length = (lax.axis_size(axis), array.shape[dim])
        up = [(i, (i + 1) % devices) for i in range(devices - 1)]
        down = [(j, i) for i, j in up]
        last = lax.slice_in_dim(array, length - width, length, axis=dim)
        leading = lax.slice_in_dim(array, 0, width, axis=dim)
        before = lax.ppermute(last, axis, up)
        after = lax.ppermute(leading, axis, down)
        array = jnp.concatenate([before, array, after], axis=dim)
    return array


def laid_out(tiles, dim):
    tiles = jnp.moveaxis(tiles, 0, dim)
    dims = tiles.shape
    return tiles.reshape(*dims[:dim], dims[dim] * dims[dim + 1], *dims[dim + 2 :])


def from_everyone(array, axis):
    copies = jnp.broadcast_to(array, (lax.axis_size(axis), *array.shape))
    return lax.all_to_all(copies, axis, split_axis=0, concat_axis=0, tiled=True)


def gathered_copies(array, axis, dim):
    return laid_out(from_everyone(array, axis), dim)


def taken_together(array, axis):
    return from_everyone(array, axis).sum(axis=0)


def gather_turned(arrays, axis, dims):
    turned = [jnp.moveaxis(a, dim, 0) for a, dim in zip(arrays, dims)]
    widths = [t[0].size for t in turned]
    both = jnp.concatenate([t.reshape(-1, w) for t, w in zip(turned, widths)], axis=1)
    result = lax.all_gather(both, axis, axis=0, tiled=True)
    tiles = jnp.split(result, [sum(widths[:k]) for k in range(1, len(widths))], axis=1)
    return tuple(
        (
            jnp.moveaxis(b.reshape(-1, *t.shape[1:]), 0, dim)
            for b, t, dim in zip(tiles, turned, dims)
        )
    )


def slot_ids(block_routes, capacity):
    flat_routes = block_routes.reshape(-1)
    hit_table = (flat_routes[:, None] == jnp.arange(EXPERTS)[None, :]).astype(jnp.int32)
    earlier = jnp.cumsum(hit_table, axis=0) - hit_table
    slot_rank = jnp.sum(earlier * hit_table, axis=1)
    return flat_routes * capacity + slot_rank


def local(
    queries,
    keys,
    values,
    sink,
    w_out,
    stream,
    gain,
    routes,
    route_weights,
    w_gate,
    w_up,
    w_down,
    shared_gate,
    shared_up,
    shared_down,
):
    tok_dev = queries.shape[0]
    n_tp = lax.axis_size("tp")
    n_sp = lax.axis_size("sp")
    tp_idx = lax.axis_index("tp")
    sp_idx = lax.axis_index("sp")
    heads_dev = HEADS // n_tp
    group = HEADS // KV_HEADS
    kv_head = tp_idx * heads_dev // group
    key_own = lax.dynamic_slice_in_dim(keys, kv_head * HD, HD, 1)
    value_own = lax.dynamic_slice_in_dim(values, kv_head * HD, HD, 1)
    paired = jnp.concatenate([key_own, value_own], axis=1)
    padded = with_halo(paired, (("sp", 0),), WINDOW)
    blocks = tok_dev // WINDOW
    framed = padded.reshape(blocks + 2, WINDOW, 2 * HD)
    banded = jnp.concatenate([framed[:-2], framed[1:-1], framed[2:]], axis=1)
    key_band = banded[:, :, :HD]
    value_band = banded[:, :, HD:]
    query_blocks = queries.reshape(blocks, WINDOW, heads_dev, HD)
    scores = jnp.einsum(
        "nqhd,njd->nhqj", query_blocks, key_band, preferred_element_type=jnp.float32
    ) * HD ** (-0.5)
    offset = sp_idx * tok_dev
    seq_total = tok_dev * n_sp
    query_pos = (
        offset + jnp.arange(blocks)[:, None, None] * WINDOW + jnp.arange(WINDOW)[None, :, None]
    )
    key_pos = (
        offset
        - WINDOW
        + jnp.arange(blocks)[:, None, None] * WINDOW
        + jnp.arange(3 * WINDOW)[None, None, :]
    )
    allowed = (jnp.abs(query_pos - key_pos) <= WINDOW) & (key_pos >= 0) & (key_pos < seq_total)
    scores = jnp.where(allowed[:, None], scores, -jnp.inf)
    sink_level = sink.reshape(1, heads_dev, 1, 1)
    row_peak = jnp.maximum(scores.max(-1, keepdims=True), sink_level)
    probabilities = jnp.exp(scores - row_peak)
    denominator = probabilities.sum(-1, keepdims=True) + jnp.exp(sink_level - row_peak)
    weights = (probabilities / denominator).astype(jnp.bfloat16)
    attended = jnp.einsum("nhqj,njd->nqhd", weights, value_band, preferred_element_type=jnp.float32)
    attended = attended.astype(jnp.bfloat16).reshape(tok_dev, heads_dev * HD)
    rows_dev = tok_dev // n_tp
    d_dev = w_down.shape[2]
    all_heads = gathered_copies(attended, "tp", 1)
    w_cols, stream_cols = (
        lax.all_to_all(w_out, "tp", split_axis=1, concat_axis=0, tiled=True),
        lax.all_to_all(stream, "tp", split_axis=1, concat_axis=0, tiled=True),
    )
    projected = jnp.dot(all_heads, w_cols, preferred_element_type=jnp.float32)
    mixed_cols = (stream_cols.astype(jnp.float32) + projected).astype(jnp.bfloat16)
    residual = mixed_cols.astype(jnp.float32)
    square_sum = taken_together(jnp.sum(residual * residual, axis=-1), "tp")
    scale_rows = lax.rsqrt(square_sum[:, None] / D + NORM_EPS)
    gain_cols = lax.dynamic_slice_in_dim(gain, tp_idx * d_dev, d_dev, 0).astype(jnp.float32)
    normed_cols = (residual * scale_rows * gain_cols[None, :]).astype(jnp.bfloat16)
    normed = gathered_copies(normed_cols, "tp", 1)
    exp_dev = w_gate.shape[0]
    capacity = max(1, 2 * tok_dev * TOPK // (n_tp * EXPERTS))
    slot_count = EXPERTS * capacity
    blocked_routes = routes.reshape(n_tp, rows_dev, TOPK)
    destination = jax.vmap(lambda block_routes: slot_ids(block_routes, capacity))(blocked_routes)
    slot_select = destination[:, None, :] == jnp.arange(slot_count)[None, :, None]
    slot_select = slot_select.reshape(n_tp, slot_count, rows_dev, TOPK).astype(jnp.float32)
    dispatch_table = jnp.sum(slot_select, axis=-1).astype(jnp.bfloat16)
    combine_table = jnp.sum(slot_select * route_weights.reshape(n_tp, 1, rows_dev, TOPK), axis=-1)
    normed_blocks = normed.reshape(n_tp, rows_dev, D)
    own_table = lax.dynamic_index_in_dim(dispatch_table, tp_idx, 0, keepdims=False)
    own_rows = lax.dynamic_index_in_dim(normed_blocks, tp_idx, 0, keepdims=False)
    outgoing = jnp.dot(own_table, own_rows, preferred_element_type=jnp.float32).astype(jnp.bfloat16)
    arrived = lax.all_to_all(outgoing, "sp", split_axis=0, concat_axis=0, tiled=True)
    arrived = arrived.reshape(1, n_sp, exp_dev, capacity, D)
    piece_rows = lax.all_gather(arrived, "tp", axis=0, tiled=True)
    gate_act = jnp.einsum(
        "tsecd,efd->tsecf", piece_rows, w_gate, preferred_element_type=jnp.float32
    )
    up_act = jnp.einsum("tsecd,efd->tsecf", piece_rows, w_up, preferred_element_type=jnp.float32)
    hidden = (jax.nn.silu(gate_act) * up_act).astype(jnp.bfloat16)
    shared_gate_act = jnp.einsum(
        "td,fd->tf", normed, shared_gate, preferred_element_type=jnp.float32
    )
    shared_up_act = jnp.einsum("td,fd->tf", normed, shared_up, preferred_element_type=jnp.float32)
    shared_hidden = (jax.nn.silu(shared_gate_act) * shared_up_act).astype(jnp.bfloat16)
    shared_hidden = shared_hidden.reshape(1, 1, 1, tok_dev, shared_hidden.shape[1])
    expert_piece, shared_piece = gather_turned((hidden, shared_hidden), "tp", (4, 4))
    piece_width = expert_piece.shape[4]
    routed_total = jnp.einsum(
        "tsecf,efd->tsecd", expert_piece, w_down, preferred_element_type=jnp.float32
    )
    shared_total = jnp.dot(
        shared_piece.reshape(tok_dev, piece_width), shared_down, preferred_element_type=jnp.float32
    )
    returned = lax.all_to_all(
        routed_total.astype(jnp.bfloat16), "sp", split_axis=1, concat_axis=1, tiled=True
    )
    returned = returned.reshape(n_tp, slot_count, d_dev).astype(jnp.float32)
    routed = jnp.einsum("tmr,tmd->trd", combine_table, returned)
    routed = routed.reshape(tok_dev, d_dev)
    return (residual + routed + shared_total).astype(jnp.bfloat16)


def solution(mesh):
    placed = (
        P("sp", "tp"),
        P("sp", None),
        P("sp", None),
        P("tp"),
        P("tp", None),
        P(("sp", "tp"), None),
        P(),
        P("sp", None),
        P("sp", None),
        P("sp", "tp", None),
        P("sp", "tp", None),
        P("sp", None, "tp"),
        P("tp", None),
        P("tp", None),
        P(None, "tp"),
    )
    return jax.shard_map(
        local, mesh=mesh, in_specs=placed, out_specs=P("sp", "tp"), check_vma=False
    )
```

profile of v0, /device:TPU:1, one launch (start us, length us, event | category | flops | bytes accessed | tf_op | source)
XLA Modules:
  0.0 313.3 jit_solution(5770819059560762188)
XLA Ops:
  6.5 1.5 copy_bitcast_fusion.1
  8.1 10.1 %all-to-all-start = ((bf16[16,16,128]{2,0,1:T(8,128)(2,1)}), bf16[16,16,128]{2,0,1:T(8,128)(2,1)S(1)}, u32[]{:S(2)}, u32[]{:S(2)}) async-start(bf16[16,16,128]{2,0,1:T(8,128)(2,1)} %copy_bitcast_fusion.1), calls=%async_computation | async-start | bytes 131072 | tf_op jit(solution)/shard_map/all_to_all | solution.py:135
  18.2 1.0 constant_dynamic-slice_fusion
  19.3 1.6 collective-permute-start
  20.9 1.3 collective-permute-start.1
  22.4 1.7 copy_bitcast_fusion
  24.8 1.0 collective-permute-done.1
  26.3 1.3 fusion.51
  27.7 8.4 %all-to-all-start.2 = ((bf16[64,16,128]{2,0,1:T(8,128)(2,1)}), bf16[64,16,128]{2,0,1:T(8,128)(2,1)S(1)}, u32[]{:S(2)}, u32[]{:S(2)}) async-start(bf16[64,16,128]{2,0,1:T(8,128)(2,1)} %copy_bitcast_fusion), calls=%async_computation.2 | async-start | bytes 524288 | tf_op jit(solution)/shard_map/all_to_all | solution.py:134
  36.2 0.2 fusion.19
  36.5 11.2 %all-to-all-done.2 = bf16[64,16,128]{2,0,1:T(8,128)(2,1)S(1)} async-done(((bf16[64,16,128]{2,0,1:T(8,128)(2,1)}), bf16[64,16,128]{2,0,1:T(8,128)(2,1)S(1)}, u32[]{:S(2)}, u32[]{:S(2)}) %all-to-all-start.2) | async-done | bytes 262176 | tf_op jit(solution)/shard_map/all_to_all | solution.py:134
  47.7 0.8 broadcast_in_dim.11
  48.6 3.5 %all-to-all-start.1 = ((bf16[16,256,64]{1,2,0:T(8,128)(2,1)}), bf16[16,256,64]{1,2,0:T(8,128)(2,1)S(1)}, u32[]{:S(2)}, u32[]{:S(2)}) async-start(bf16[16,256,64]{1,2,0:T(8,128)(2,1)} %broadcast_in_dim.11), calls=%async_computation.1 | async-start | bytes 1048576 | tf_op jit(solution)/shard_map/all_to_all | solution.py:39
  52.2 16.6 %all-to-all-done.1 = bf16[16,256,64]{1,2,0:T(8,128)(2,1)S(1)} async-done(((bf16[16,256,64]{1,2,0:T(8,128)(2,1)}), bf16[16,256,64]{1,2,0:T(8,128)(2,1)S(1)}, u32[]{:S(2)}, u32[]{:S(2)}) %all-to-all-start.1) | async-done | bytes 524320 | tf_op jit(solution)/shard_map/all_to_all | solution.py:39
  68.8 0.3 multiply_reduce_fusion
  69.1 0.6 broadcast_in_dim.12
  69.7 3.4 %all-to-all-start.3 = ((f32[16,1,256]{2,1,0:T(1,128)}), f32[16,1,256]{2,1,0:T(1,128)S(1)}, u32[]{:S(2)}, u32[]{:S(2)}) async-start(f32[16,1,256]{2,1,0:T(1,128)} %broadcast_in_dim.12), calls=%async_computation.3 | async-start | bytes 32768 | tf_op jit(solution)/shard_map/all_to_all | solution.py:39
  73.1 0.8 dynamic-slice_convert_fusion.1
  73.9 6.2 %all-to-all-done.3 = f32[16,1,256]{2,1,0:T(1,128)S(1)} async-done(((f32[16,1,256]{2,1,0:T(1,128)}), f32[16,1,256]{2,1,0:T(1,128)S(1)}, u32[]{:S(2)}, u32[]{:S(2)}) %all-to-all-start.3) | async-done | bytes 16416 | tf_op jit(solution)/shard_map/all_to_all | solution.py:39
  80.2 1.1 broadcast_in_dim.13
  81.3 3.8 %all-to-all-start.4 = ((bf16[16,256,128]{1,2,0:T(8,128)(2,1)}), bf16[16,256,128]{1,2,0:T(8,128)(2,1)S(1)}, u32[]{:S(2)}, u32[]{:S(2)}) async-start(bf16[16,256,128]{1,2,0:T(8,128)(2,1)} %broadcast_in_dim.13), calls=%async_computation.4 | async-start | bytes 2097152 | tf_op jit(solution)/shard_map/all_to_all | solution.py:39
  85.7 1.4 select_reduce_fusion.1
  87.3 1.0 select_reduce_fusion
  88.3 24.9 %all-to-all-done.4 = bf16[16,256,128]{1,2,0:T(8,128)(2,1)S(1)} async-done(((bf16[16,256,128]{1,2,0:T(8,128)(2,1)}), bf16[16,256,128]{1,2,0:T(8,128)(2,1)S(1)}, u32[]{:S(2)}, u32[]{:S(2)}) %all-to-all-start.4) | async-done | bytes 1048608 | tf_op jit(solution)/shard_map/all_to_all | solution.py:39
  113.2 1.1 copy.141
  114.2 1.3 reshape_reshape.2
  115.5 1.2 convolution_convert_fusion
  116.7 0.2 all_to_all.49
  116.9 32.0 %all_to_all.59 = bf16[32,4,2048]{2,1,0:T(4,128)(2,1)S(1)} all-to-all(bf16[32,4,2048]{2,1,0:T(4,128)(2,1)S(1)} %all_to_all.49), channel_id=1, replica_groups=mesh['sp'=32,'tp'=16] {'sp'}, dimensions={0} | all-to-all | bytes 1048576 | tf_op jit(solution)/shard_map/all_to_all | solution.py:158
  148.9 1.1 copy.142
  150.1 0.2 all-gather.5.cloned.1.call-start
  150.3 0.3 fusion.52
  150.6 1.2 fusion.18
  152.0 49.5 %all-gather.3.cloned.1.call-done = bf16[16,32,2,2,2048]{4,1,3,0,2:T(8,128)(2,1)} async-done(((bf16[1,32,2,2,2048]{4,1,3,0,2:T(8,128)(2,1)}), bf16[16,32,2,2,2048]{4,1,3,0,2:T(8,128)(2,1)}) %all-gather.3.cloned.1.call-update) | async-done | bytes 8388624 | tf_op jit(solution)/shard_map/all_gather | solution.py:160
  201.5 5.8 %convolution_bitcast_fusion.1 = f32[64,16,32,2,2]{0,2,4,1,3:T(8,128)S(1)} fusion(bf16[16,32,2,2,2048]{4,1,3,0,2:T(8,128)(2,1)} %all-gather.3.cloned.1.call-done, bf16[2,64,2048]{2,1,0:T(8,128)(2,1)S(1)} %copy-done.2), kind=kOutput, calls=%fused_computation.6 | convolution fusion | flops 536870912 | bytes 9437184 | tf_op jit(solution)/shard_map/tsecd,efd->tsecf/dot_general | solution.py:161
  207.4 2.3 fusion.4
  209.7 0.5 copy.143
  210.3 1.0 copy.145
  211.3 43.6 %all-gather.5.cloned.1.call-done = bf16[1024,2304]{1,0:T(8,128)(2,1)} async-done(((bf16[64,2304]{1,0:T(8,128)(2,1)}), bf16[1024,2304]{1,0:T(8,128)(2,1)}) %all-gather.5.cloned.1.call-update) | async-done | bytes 4718608 | tf_op jit(solution)/shard_map/all_gather | solution.py:54
  255.0 4.8 %split.8 = bf16[1024,2048]{1,0:T(8,128)(2,1)} slice(bf16[1024,2304]{1,0:T(8,128)(2,1)} %all-gather.5.cloned.1.call-done), slice={[0:1024], [0:2048]} | slice | bytes 8388608 | tf_op jit(solution)/shard_map/split | solution.py:55
  259.8 6.5 %copy.146 = bf16[1024,2048]{0,1:T(8,128)(2,1)} copy(bf16[1024,2048]{1,0:T(8,128)(2,1)} %split.8) | data formatting | bytes 8388608 | tf_op jit(solution)/shard_map/split | solution.py:55
  266.3 7.2 %reshape.237 = bf16[1024,16,32,2,2]{0,4,3,2,1:T(2,128)(2,1)} reshape(bf16[1024,2048]{0,1:T(8,128)(2,1)} %copy.146) | data formatting | bytes 8388608 | tf_op jit(solution)/shard_map/reshape | solution.py:58
  273.5 3.6 %fusion.8 = bf16[16,32,2,2,128]{4,1,3,0,2:T(8,128)(2,1)S(1)} fusion(bf16[1024,16,32,2,2]{0,4,3,2,1:T(2,128)(2,1)} %reshape.237, bf16[2,1024,128]{2,1,0:T(8,128)(2,1)S(1)} %copy-done), kind=kOutput, calls=%fused_computation.9 | convolution fusion | flops 537133056 | bytes 5242880 | tf_op jit(solution)/shard_map/tsecf,efd->tsecd/dot_general | solution.py:174
  277.0 0.5 copy.148
  277.6 26.3 %all_to_all.60 = bf16[16,32,2,2,128]{4,3,0,2,1:T(2,128)(2,1)S(1)} all-to-all(bf16[16,32,2,2,128]{4,3,0,2,1:T(2,128)(2,1)S(1)} %copy.148), channel_id=1, replica_groups=mesh['sp'=32,'tp'=16] {'sp'}, dimensions={1} | all-to-all | bytes 1048576 | tf_op jit(solution)/shard_map/all_to_all | solution.py:180
  304.0 0.3 fusion.28
  304.4 1.3 fusion.16
  305.7 0.7 copy.153
  (58 shorter events, 2.4 us)
Async XLA Ops:
  6.5 266.9 %copy-start = (bf16[2,1024,128]{2,1,0:T(8,128)(2,1)S(1)}, bf16[2,1024,128]{2,1,0:T(8,128)(2,1)}, u32[]{:S(2)}) copy-start(bf16[2,1024,128]{2,1,0:T(8,128)(2,1)} %param.26) | copy-start | bytes 1572868
  8.1 19.6 %all-to-all-start = ((bf16[16,16,128]{2,0,1:T(8,128)(2,1)}), bf16[16,16,128]{2,0,1:T(8,128)(2,1)S(1)}, u32[]{:S(2)}, u32[]{:S(2)}) async-start(bf16[16,16,128]{2,0,1:T(8,128)(2,1)} %copy_bitcast_fusion.1), calls=%async_computation | async-start | bytes 131072 | tf_op jit(solution)/shard_map/all_to_all | solution.py:135
  19.3 5.5 %collective-permute-start = (bf16[128,128]{1,0:T(8,128)(2,1)S(1)}, bf16[128,128]{1,0:T(8,128)(2,1)S(1)}, u32[]{:S(2)}, u32[]{:S(2)}) collective-permute-start(bf16[128,128]{1,0:T(8,128)(2,1)S(1)} %get-tuple-element.10), channel_id=1, source_target_pairs={{0,16},{16,32},{32,48},{48,64},{64,80},{80,96},{96,112},{112,128},... | collective-permute-start | bytes 98312 | tf_op jit(solution)/shard_map/ppermute | solution.py:25
  20.9 4.9 %collective-permute-start.1 = (bf16[128,128]{1,0:T(8,128)(2,1)S(1)}, bf16[128,128]{1,0:T(8,128)(2,1)S(1)}, u32[]{:S(2)}, u32[]{:S(2)}) collective-permute-start(bf16[128,128]{1,0:T(8,128)(2,1)S(1)} %get-tuple-element.11), channel_id=1, source_target_pairs={{16,0},{32,16},{48,32},{64,48},{80,64},{96,80},{112,96},{128,112},... | collective-permute-start | bytes 98312 | tf_op jit(solution)/shard_map/ppermute | solution.py:26
  27.7 57.5 %copy-start.6 = (s32[256,4]{0,1:T(4,128)S(1)}, s32[256,4]{0,1:T(4,128)}, u32[]{:S(2)}) copy-start(s32[256,4]{0,1:T(4,128)} %param.22) | copy-start | bytes 12292
  27.7 57.7 %copy-start.7 = (f32[256,4]{0,1:T(4,128)S(1)}, f32[256,4]{0,1:T(4,128)}, u32[]{:S(2)}) copy-start(f32[256,4]{0,1:T(4,128)} %param.23) | copy-start | bytes 12292
  27.7 20.0 %all-to-all-start.2 = ((bf16[64,16,128]{2,0,1:T(8,128)(2,1)}), bf16[64,16,128]{2,0,1:T(8,128)(2,1)S(1)}, u32[]{:S(2)}, u32[]{:S(2)}) async-start(bf16[64,16,128]{2,0,1:T(8,128)(2,1)} %copy_bitcast_fusion), calls=%async_computation.2 | async-start | bytes 524288 | tf_op jit(solution)/shard_map/all_to_all | solution.py:134
  48.6 20.2 %all-to-all-start.1 = ((bf16[16,256,64]{1,2,0:T(8,128)(2,1)}), bf16[16,256,64]{1,2,0:T(8,128)(2,1)S(1)}, u32[]{:S(2)}, u32[]{:S(2)}) async-start(bf16[16,256,64]{1,2,0:T(8,128)(2,1)} %broadcast_in_dim.11), calls=%async_computation.1 | async-start | bytes 1048576 | tf_op jit(solution)/shard_map/all_to_all | solution.py:39
  69.7 10.3 %all-to-all-start.3 = ((f32[16,1,256]{2,1,0:T(1,128)}), f32[16,1,256]{2,1,0:T(1,128)S(1)}, u32[]{:S(2)}, u32[]{:S(2)}) async-start(f32[16,1,256]{2,1,0:T(1,128)} %broadcast_in_dim.12), calls=%async_computation.3 | async-start | bytes 32768 | tf_op jit(solution)/shard_map/all_to_all | solution.py:39
  81.3 31.9 %all-to-all-start.4 = ((bf16[16,256,128]{1,2,0:T(8,128)(2,1)}), bf16[16,256,128]{1,2,0:T(8,128)(2,1)S(1)}, u32[]{:S(2)}, u32[]{:S(2)}) async-start(bf16[16,256,128]{1,2,0:T(8,128)(2,1)} %broadcast_in_dim.13), calls=%async_computation.4 | async-start | bytes 2097152 | tf_op jit(solution)/shard_map/all_to_all | solution.py:39
  85.1 116.4 %all-gather.3.cloned.1.call-start = ((), (), s32[]{:S(2)}) async-start(), calls=%async_computation.7 | async-start | bytes 8912896 | tf_op jit(solution)/shard_map/all_gather | solution.py:160
  85.2 65.1 %copy-start.4 = (bf16[64,2048]{1,0:T(8,128)(2,1)S(1)}, bf16[64,2048]{1,0:T(8,128)(2,1)}, u32[]{:S(2)}) copy-start(bf16[64,2048]{1,0:T(8,128)(2,1)} %param.27) | copy-start | bytes 786436
  114.2 87.3 %copy-start.2 = (bf16[2,64,2048]{2,1,0:T(8,128)(2,1)S(1)}, bf16[2,64,2048]{2,1,0:T(8,128)(2,1)}, u32[]{:S(2)}) copy-start(bf16[2,64,2048]{2,1,0:T(8,128)(2,1)} %param.24) | copy-start | bytes 1572868
  150.1 104.9 %all-gather.5.cloned.1.call-start = ((), (), s32[]{:S(2)}) async-start(), calls=%async_computation.8 | async-start | bytes 5013504 | tf_op jit(solution)/shard_map/all_gather | solution.py:54
  152.0 55.4 %copy-start.8 = (bf16[2,64,2048]{2,1,0:T(8,128)(2,1)S(1)}, bf16[2,64,2048]{2,1,0:T(8,128)(2,1)}, u32[]{:S(2)}) copy-start(bf16[2,64,2048]{2,1,0:T(8,128)(2,1)} %param.25) | copy-start | bytes 1572868
  201.5 5.9 %copy-start.1 = (bf16[16,32,2,2,2048]{4,1,3,0,2:T(8,128)(2,1)S(1)}, bf16[16,32,2,2,2048]{4,1,3,0,2:T(8,128)(2,1)}, u32[]{:S(2)}) copy-start(bf16[16,32,2,2,2048]{4,1,3,0,2:T(8,128)(2,1)} %all-gather.3.cloned.1.call-done) | copy-start | bytes 25165828
  273.5 30.5 %copy-start.5 = (bf16[16,128,16]{1,2,0:T(8,128)(2,1)S(1)}, bf16[16,128,16]{1,2,0:T(8,128)(2,1)}, u32[]{:S(2)}) copy-start(bf16[16,128,16]{1,2,0:T(8,128)(2,1)} %get-tuple-element.5) | copy-start | bytes 196612
  273.5 30.9 %copy-start.3 = (bf16[1024,128]{1,0:T(8,128)(2,1)S(1)}, bf16[1024,128]{1,0:T(8,128)(2,1)}, u32[]{:S(2)}) copy-start(bf16[1024,128]{1,0:T(8,128)(2,1)} %param.29) | copy-start | bytes 786436
Sparse Core Ops, SparseCore 0:
  150.2 51.2 all-gather.2
  211.5 43.4 all-gather.4
where the time goes:
time: 315 us; the launch traced here: 313 us
  waiting for transfers between devices  153 us (49%)
  blocking collectives  58.3 us (19%)
  local copies, waits for them, and re-layouts  33.1 us (11%)
  starting transfers between devices  32.4 us (10%)
  matrix products  17.8 us (6%)
  between operations  14.5 us (5%)
  other arithmetic  4.02 us (1%)
    all_gather x1, waiting for transfers between devices, local(): piece_rows = lax.all_gather(arrived, 'tp', axis=0, tiled=True)  49.5 us
    all_to_all x3, waiting for transfers between devices, from_everyone(): return lax.all_to_all(copies, axis, split_axis=0, concat_axis=0, tiled=True)  47.7 us
    all_gather x1, waiting for transfers between devices, gather_turned(): result = lax.all_gather(both, axis, axis=0, tiled=True)  43.6 us
    all_to_all x1, blocking collectives, local(): lax.all_to_all(outgoing, 'sp', split_axis=0, concat_axis=0, tiled=True)  32 us
    all_to_all x1, blocking collectives, local(): lax.all_to_all(routed_total.astype(jnp.bfloat16), 'sp', split_axis=1, con...  26.3 us
    split x2, local copies, waits for them, and re-layouts, gather_turned(): jnp.split(result, [sum(widths[:k]) for k in range(1, len(widths))], axis=1)  11.3 us
    all_to_all x1, waiting for transfers between devices, local(): lax.all_to_all(w_out, 'tp', split_axis=1, concat_axis=0, tiled=True)  11.2 us
    all_to_all x3, starting transfers between devices, from_everyone(): return lax.all_to_all(copies, axis, split_axis=0, concat_axis=0, tiled=True)  10.7 us
  transfers between devices with their start and end apart: 9, of which 7 were waited for; matrix products, arithmetic and copies ran while one was open for 3% of the time, Pallas kernels for 0%

commit v1 on v0

v1 whole, which is shorter than its diff:
```python
import functools

import jax
import jax.numpy as jnp
from jax import lax
from jax.experimental import pallas as pl
from jax.experimental.pallas import tpu as pltpu
from jax.sharding import PartitionSpec as P

HD = 64
WINDOW = 128
CAP = 2
NX = 4
Z_ORDER = (0, 1, 4, 5, 3, 6, 2, 7)
NORM_EPS = 1e-05
BF = jnp.bfloat16
F32 = jnp.float32

NT = (((1,), (1,)), ((), ()))
TN = (((0,), (0,)), ((), ()))


def dot(a, b, dims=(((1,), (0,)), ((), ()))):
    return lax.dot_general(a, b, dims, preferred_element_type=F32)


def kernel(
    q_ref,
    k_ref,
    v_ref,
    sink_ref,
    w_out_ref,
    stream_ref,
    gain_ref,
    routes_ref,
    rw_ref,
    w_gate_ref,
    w_up_ref,
    w_down_ref,
    sg_ref,
    su_ref,
    sd_ref,
    out_ref,
    wcol,
    scol,
    halo,
    abuf,
    sbuf,
    gbuf,
    obuf,
    hs,
    hbuf,
    ybuf,
    rbuf,
    ptab,
    ctab,
    stab,
    wexp,
    wdt,
    resid,
    shared_out,
    w_sem,
    st_sem,
    halo_send,
    halo_recv,
    a_send,
    a_recv,
    d_send,
    d_recv,
    r_send,
    r_recv,
    ts_send,
    ts_recv,
    t_send,
    t_recv,
    hs_send,
    hs_recv,
    h_send,
    h_recv,
    *,
    kv_group,
    order,
    nx,
):
    tok, hd = q_ref.shape
    d_model = stream_ref.shape[1]
    rows_dev = stream_ref.shape[0]
    n_tp = lax.axis_size("tp")
    n_sp = lax.axis_size("sp")
    ny = n_tp // 2
    nz = n_sp // nx
    dc = d_model // n_tp
    exp_dev, fh = w_gate_ref.shape[0], w_gate_ref.shape[1]
    experts = exp_dev * n_sp
    topk = routes_ref.shape[0]
    slots = n_tp * CAP
    n_chunk = len(order) // 2 if len(order) > 2 else len(order)
    zc = len(order) // n_chunk
    crow = zc * nx * slots
    sp = lax.axis_index("sp")
    tp = lax.axis_index("tp")
    y, c = tp // 2, tp % 2
    z, x = sp // nx, sp % nx
    half = ny // 2

    def cols(t):
        return pl.ds(pl.multiple_of(t * dc, dc), dc)

    def units(t):
        return pl.ds(pl.multiple_of(t * fh, fh), fh)

    def chip(dy):
        return lax.rem(y + dy + ny, ny)

    def remote(src, dst, send, recv, **device):
        return pltpu.make_async_remote_copy(
            src_ref=src,
            dst_ref=dst,
            send_sem=send,
            recv_sem=recv,
            device_id=device,
            device_id_type=pl.DeviceIdType.MESH,
        )

    def wait_for(ref, sem):
        pltpu.make_async_copy(ref, ref, sem).wait()

    barrier = pltpu.get_barrier_semaphore()

    def greet_tp(i, carry):
        pl.semaphore_signal(barrier, inc=1, device_id={"tp": lax.rem(tp + i, n_tp)})
        return carry

    def greet_sp(i, carry):
        pl.semaphore_signal(barrier, inc=1, device_id={"sp": lax.rem(sp + i, n_sp)})
        return carry

    lax.fori_loop(1, n_tp, greet_tp, 0)
    lax.fori_loop(1, n_sp, greet_sp, 0)

    row_e = lax.broadcasted_iota(jnp.int32, (experts, tok), 0)
    hit_t = jnp.zeros((experts, tok), F32)
    weight_t = jnp.zeros((experts, tok), F32)
    for k in range(topk):
        hit = row_e == routes_ref[k : k + 1, :]
        hit_t = jnp.where(hit, 1.0, hit_t)
        weight_t = jnp.where(hit, rw_ref[k : k + 1, :], weight_t)
    early = lax.broadcasted_iota(jnp.int32, (tok, tok), 0)
    late = lax.broadcasted_iota(jnp.int32, (tok, tok), 1)
    before = (early < late) & (early // rows_dev == late // rows_dev)
    rank_t = dot(hit_t.astype(BF), jnp.where(before, 1.0, 0.0).astype(BF))
    slot_t = jnp.where(hit_t > 0, rank_t, -1.0)
    stab[...] = slot_t
    slot_row = lax.broadcasted_iota(jnp.int32, (slots, tok), 0)
    slot_tok = lax.broadcasted_iota(jnp.int32, (slots, tok), 1)
    in_block = (slot_row // CAP) == (slot_tok // rows_dev)
    slot_rank = jnp.where(in_block, slot_row % CAP, -2).astype(F32)

    def table_rows(e, carry):
        line = stab[pl.ds(e, 1), :]
        ptab[pl.ds(pl.multiple_of(e * slots, slots), slots), :] = jnp.where(
            line == slot_rank, 1.0, 0.0
        ).astype(BF)
        return carry

    lax.fori_loop(0, experts, table_rows, 0)

    pl.semaphore_wait(barrier, n_tp - 1 + n_sp - 1)

    head_kv = tp // kv_group
    pair = pl.ds(pl.multiple_of((head_kv // 2) * 2 * hd, 2 * hd), 2 * hd)
    last, first = sp == n_sp - 1, sp == 0
    to_next = lax.rem(sp + 1, n_sp)
    to_prev = lax.rem(sp + n_sp - 1, n_sp)

    def halo_copy(i):
        src = (k_ref, v_ref)[i % 2]
        rows = pl.ds(tok - WINDOW, WINDOW) if i < 2 else pl.ds(0, WINDOW)
        return remote(
            src.at[rows, pair],
            halo.at[i],
            halo_send.at[i],
            halo_recv.at[i],
            sp=to_next if i < 2 else to_prev,
        )

    @pl.when(jnp.logical_not(last))
    def _():
        halo_copy(0).start()
        halo_copy(1).start()

    @pl.when(jnp.logical_not(first))
    def _():
        halo_copy(2).start()
        halo_copy(3).start()

    def send_cols(i, carry):
        t = lax.rem(tp + i, n_tp)
        remote(w_out_ref.at[:, cols(t)], wcol.at[tp], w_sem.at[0], w_sem.at[1], tp=t).start()
        remote(stream_ref.at[:, cols(t)], scol.at[tp], st_sem.at[0], st_sem.at[1], tp=t).start()
        return carry

    lax.fori_loop(1, n_tp, send_cols, 0)
    wcol[tp] = w_out_ref[:, cols(tp)]
    scol[tp] = stream_ref[:, cols(tp)]

    @pl.when(first)
    def _():
        halo[0] = jnp.zeros(halo.shape[1:], BF)
        halo[1] = jnp.zeros(halo.shape[1:], BF)

    @pl.when(last)
    def _():
        halo[2] = jnp.zeros(halo.shape[1:], BF)
        halo[3] = jnp.zeros(halo.shape[1:], BF)

    @pl.when(jnp.logical_not(first))
    def _():
        halo_copy(0).wait_recv()
        halo_copy(1).wait_recv()

    @pl.when(jnp.logical_not(last))
    def _():
        halo_copy(2).wait_recv()
        halo_copy(3).wait_recv()

    odd = head_kv % 2
    lane = lax.broadcasted_iota(jnp.int32, (tok, 2 * hd), 1)
    query = q_ref[...]
    query = jnp.concatenate([query, query], axis=1)
    query = jnp.where(lane // hd == odd, query, jnp.zeros_like(query))
    sink = sink_ref[0:1, 0:1]
    key_i = lax.broadcasted_iota(jnp.int32, (WINDOW, WINDOW), 0)
    query_i = lax.broadcasted_iota(jnp.int32, (WINDOW, WINDOW), 1)
    blocks = tok // WINDOW
    for n in range(blocks):
        q_n = query[n * WINDOW : (n + 1) * WINDOW]
        parts = []
        for j in (-1, 0, 1):
            b = n + j
            if b < 0:
                key, value = halo[0], halo[1]
                allowed = (query_i <= key_i) & jnp.logical_not(first)
            elif b == blocks:
                key, value = halo[2], halo[3]
                allowed = (key_i <= query_i) & jnp.logical_not(last)
            else:
                rows = pl.ds(b * WINDOW, WINDOW)
                key, value = k_ref[rows, pair], v_ref[rows, pair]
                allowed = (query_i <= key_i, None, key_i <= query_i)[j + 1]
            score = dot(key, q_n, NT) * (hd**-0.5)
            if allowed is not None:
                score = jnp.where(allowed, score, -jnp.inf)
            parts.append((score, value))
        peak = jnp.maximum(sink, jnp.max(parts[0][0], axis=0, keepdims=True))
        for score, _v in parts[1:]:
            peak = jnp.maximum(peak, jnp.max(score, axis=0, keepdims=True))
        exps = [jnp.exp(score - peak) for score, _v in parts]
        total = jnp.exp(sink - peak)
        for e in exps:
            total = total + jnp.sum(e, axis=0, keepdims=True)
        mix = None
        for e, (_s, value) in zip(exps, parts):
            prob = (e / total).astype(BF)
            term = dot(value, prob, TN)
            mix = term if mix is None else mix + term
        mine = jnp.where(odd == 0, mix[:hd], mix[hd:])
        abuf[tp, :, n * WINDOW : (n + 1) * WINDOW] = mine.astype(BF)

    def peer_of(t):
        return 2 * (t // 2) + 1 - t % 2

    partner = peer_of(tp)

    def to_partner(t):
        return remote(abuf.at[t], abuf.at[t], a_send, a_recv.at[t], tp=partner)

    far = []
    for h in range(half, 0, -1):
        far.append(h)
        if h != half:
            far.append(-h)
    for h in far:
        remote(
            abuf.at[tp], abuf.at[tp], a_send, a_recv.at[tp], tp=2 * chip(h) + c
        ).start()
    to_partner(tp).start()

    gain = gain_ref[...].astype(F32)
    for e in range(exp_dev):
        wexp[e, :fh, :] = (w_gate_ref[e].astype(F32) * gain).astype(BF)
        wexp[e, fh:, :] = (w_up_ref[e].astype(F32) * gain).astype(BF)
    wexp[exp_dev, :fh, :] = (sg_ref[...].astype(F32) * gain).astype(BF)
    wexp[exp_dev, fh:, :] = (su_ref[...].astype(F32) * gain).astype(BF)

    for h in reversed(far):
        t = 2 * chip(h) + c
        wait_for(abuf.at[t], a_recv.at[t])
        to_partner(t).start()

    for e in range(exp_dev):
        wdt[e] = w_down_ref[e].astype(F32).T.astype(BF)
    wdt[exp_dev] = sd_ref[...].astype(F32).T.astype(BF)

    wait_for(wcol.at[pl.ds(0, n_tp - 1)], w_sem.at[1])
    wait_for(scol.at[pl.ds(0, n_tp - 1)], st_sem.at[1])
    for i in range(ny):
        t = 2 * chip(i) + 1 - c
        wait_for(abuf.at[t], a_recv.at[t])
    projected = dot(
        abuf[...].reshape(n_tp * hd, tok), wcol[...].reshape(n_tp * hd, dc), TN
    )
    mixed = (scol[...].reshape(tok, dc).astype(F32) + projected).astype(BF)
    resid[...] = mixed
    sbuf[:, cols(tp)] = mixed

    def dest(i, j):
        return lax.rem(z - order[i] + nz, nz) * nx + lax.rem(x + j, nx)

    def source(i, j):
        return lax.rem(z + order[i], nz) * nx + lax.rem(x + j, nx)

    def spot(pos):
        return pl.ds(pl.multiple_of(pos * slots, slots), slots)

    def chunk_rows(k):
        return pl.ds(pl.multiple_of(k * crow, crow), crow)

    pieces = min(4, n_sp)
    span = experts // pieces
    for part in range(pieces):
        rows = dot(ptab[part * span * slots : (part + 1) * span * slots, :], mixed)
        count = span // exp_dev
        obuf[part * count : (part + 1) * count] = rows.astype(BF).reshape(
            count, exp_dev, slots, dc
        )

    def ring_start(block, send, recv):
        for t in (2 * chip(1) + c, 2 * chip(-1) + c, partner):
            remote(block(tp), block(tp), send, recv(tp), tp=t).start()

    def ring_hop(block, send, recv, h):
        for sign in (1, -1):
            if h == half and sign == -1:
                continue
            t = 2 * chip(-sign * h) + c
            wait_for(block(t), recv(t))
            onto = 2 * chip(sign) + c
            if h < half - 1:
                remote(block(t), block(t), send, recv(t), tp=onto).start()
            elif h == half - 1:

                @pl.when(c == (0 if sign == 1 else 1))
                def _():
                    remote(block(t), block(t), send, recv(t), tp=onto).start()

            remote(block(t), block(t), send, recv(t), tp=partner).start()

    def ring_end(block, recv):
        for i in range(ny):
            t = 2 * chip(i) + 1 - c
            wait_for(block(t), recv(t))

    tok_shared = (
        lambda t: sbuf.at[:, cols(t)],
        ts_send,
        lambda t: ts_recv.at[t],
    )
    hid_shared = (
        lambda t: hs.at[units(t), :],
        hs_send,
        lambda t: hs_recv.at[t],
    )

    def tok_ring(k):
        return (
            lambda t: gbuf.at[:, chunk_rows(k), cols(t)],
            t_send.at[k],
            lambda t: t_recv.at[k, t],
        )

    def hid_ring(k):
        return (
            lambda t: hbuf.at[:, units(t), chunk_rows(k)],
            h_send.at[k],
            lambda t: h_recv.at[k, t],
        )

    def send_rows(i, j):
        d = dest(i, j)
        return remote(
            obuf.at[d],
            gbuf.at[:, spot(i * nx + x), cols(tp)],
            d_send,
            d_recv.at[i // zc],
            sp=d,
        )

    for i in range(len(order)):
        for j in range(nx):
            if i or j:
                send_rows(i, j).start()
    gbuf[:, spot(x), cols(tp)] = obuf[sp]
    ring_start(*tok_shared)

    def rows_arrived(k):
        count = zc * nx - (1 if k == 0 else 0)
        wait_for(
            gbuf.at[:, pl.ds(0, count * slots), cols(tp)],
            d_recv.at[k],
        )

    slot_c = slot_t.T.astype(BF)
    weight_c = weight_t.T.astype(BF)
    width = min(512, experts * slots)
    for part in range(experts * slots // width):
        m = lax.broadcasted_iota(jnp.int32, (experts, width), 1) + part * width
        e_i = lax.broadcasted_iota(jnp.int32, (experts, width), 0)
        spread = jnp.where(m // slots == e_i, 1.0, 0.0).astype(BF)
        m2 = lax.broadcasted_iota(jnp.int32, (tok, width), 1) + part * width
        r2 = lax.broadcasted_iota(jnp.int32, (tok, width), 0)
        want = jnp.where((m2 % slots) // CAP == r2 // rows_dev, m2 % CAP, -2).astype(F32)
        table = jnp.where(dot(slot_c, spread) == want, dot(weight_c, spread), 0.0)
        ctab[:, part * width : (part + 1) * width] = table.astype(BF)

    def hidden_of(rows, e):
        wide = rows.astype(F32)
        squares = wide * wide
        part = squares[:, :128]
        for i in range(1, d_model // 128):
            part = part + squares[:, i * 128 : (i + 1) * 128]
        total = jnp.sum(part.T, axis=0, keepdims=True)
        scale = lax.rsqrt(total / d_model + NORM_EPS)
        acts = dot(wexp[e], rows, NT) * scale
        gate, up = acts[:fh], acts[fh:]
        return (gate / (1.0 + jnp.exp(-gate)) * up).astype(BF)

    def up_shared():
        hs[units(tp), :] = hidden_of(sbuf[...], exp_dev)

    def up_chunk(k):
        for e in range(exp_dev):
            hbuf[e, units(tp), chunk_rows(k)] = hidden_of(gbuf[e, chunk_rows(k), :], e)

    def down_chunk(k):
        for e in range(exp_dev):
            res = dot(wdt[e], hbuf[e, :, chunk_rows(k)])
            ybuf[e, chunk_rows(k), :] = res.T.astype(BF)

    def give_back(i, j):
        s = source(i, j)
        pos = i * nx + lax.rem(x + j, nx)
        return remote(ybuf.at[:, spot(pos), :], rbuf.at[sp], r_send, r_recv, sp=s)

    def return_chunk(k):
        for i in range(k * zc, (k + 1) * zc):
            for j in range(nx):
                if i or j:
                    give_back(i, j).start()
        if k == 0:
            rbuf[sp] = ybuf[:, spot(x), :]

    ring_hop(*tok_shared, 1)
    rows_arrived(0)
    ring_start(*tok_ring(0))
    for h in range(2, half + 1):
        ring_hop(*tok_shared, h)
        ring_hop(*tok_ring(0), h - 1)
    rows_arrived(1)
    ring_start(*tok_ring(1))
    ring_end(tok_shared[0], tok_shared[2])
    up_shared()
    ring_start(*hid_shared)
    ring_hop(*tok_ring(0), half)
    ring_end(tok_ring(0)[0], tok_ring(0)[2])
    up_chunk(0)
    ring_start(*hid_ring(0))
    for k in range(1, n_chunk):
        for h in range(1, half + 1):
            ring_hop(*tok_ring(k), h)
            if k == 1:
                ring_hop(*hid_shared, h)
            ring_hop(*hid_ring(k - 1), h)
        if k + 1 < n_chunk:
            rows_arrived(k + 1)
            ring_start(*tok_ring(k + 1))
        ring_end(tok_ring(k)[0], tok_ring(k)[2])
        up_chunk(k)
        ring_start(*hid_ring(k))
        ring_end(hid_ring(k - 1)[0], hid_ring(k - 1)[2])
        down_chunk(k - 1)
        return_chunk(k - 1)
        if k == 1:
            ring_end(hid_shared[0], hid_shared[2])
            shared_out[...] = dot(wdt[exp_dev], hs[...]).T
    for h in range(1, half + 1):
        ring_hop(*hid_ring(n_chunk - 1), h)
    ring_end(hid_ring(n_chunk - 1)[0], hid_ring(n_chunk - 1)[2])
    down_chunk(n_chunk - 1)
    return_chunk(n_chunk - 1)

    wait_for(wcol.at[pl.ds(0, n_tp - 1)], w_sem.at[0])
    wait_for(scol.at[pl.ds(0, n_tp - 1)], st_sem.at[0])

    @pl.when(jnp.logical_not(last))
    def _():
        halo_copy(0).wait_send()
        halo_copy(1).wait_send()

    @pl.when(jnp.logical_not(first))
    def _():
        halo_copy(2).wait_send()
        halo_copy(3).wait_send()

    wait_for(abuf.at[pl.ds(0, n_tp - 1)], a_send)
    wait_for(obuf.at[pl.ds(0, n_sp - 1)], d_send)
    wait_for(sbuf.at[:, pl.ds(0, (n_tp - 1) * dc)], ts_send)
    wait_for(hs.at[pl.ds(0, (n_tp - 1) * fh), :], hs_send)
    for k in range(n_chunk):
        wait_for(gbuf.at[:, chunk_rows(k), pl.ds(0, (n_tp - 1) * dc)], t_send.at[k])
        wait_for(hbuf.at[:, pl.ds(0, (n_tp - 1) * fh), chunk_rows(k)], h_send.at[k])
    wait_for(rbuf.at[pl.ds(0, n_sp - 1)], r_send)

    wait_for(rbuf.at[pl.ds(0, n_sp - 1)], r_recv)
    routed = dot(ctab[...], rbuf[...].reshape(experts * slots, dc))
    out_ref[...] = (resid[...].astype(F32) + routed + shared_out[...]).astype(BF)


def local(
    queries,
    keys,
    values,
    sink,
    w_out,
    stream,
    gain,
    routes,
    route_weights,
    w_gate,
    w_up,
    w_down,
    shared_gate,
    shared_up,
    shared_down,
    *,
    kv_group,
    order,
    nx,
):
    n_tp = lax.axis_size("tp")
    n_sp = lax.axis_size("sp")
    tok = queries.shape[0]
    rows, d_model = stream.shape
    dc = d_model // n_tp
    exp_dev, fh, _ = w_gate.shape
    experts = exp_dev * n_sp
    slots = n_tp * CAP
    n_rows = n_sp * slots
    n_chunk = len(order) // 2 if len(order) > 2 else len(order)
    vm = pltpu.VMEM
    dma = pltpu.SemaphoreType.DMA
    return pl.pallas_call(
        functools.partial(kernel, kv_group=kv_group, order=order, nx=nx),
        out_shape=jax.ShapeDtypeStruct((tok, dc), BF),
        in_specs=[pl.BlockSpec(memory_space=vm)] * 15,
        out_specs=pl.BlockSpec(memory_space=vm),
        scratch_shapes=[
            vm((n_tp, w_out.shape[0], dc), BF),
            vm((n_tp, rows, dc), BF),
            vm((4, WINDOW, 2 * HD), BF),
            vm((n_tp, HD, tok), BF),
            vm((tok, d_model), BF),
            vm((exp_dev, n_rows, d_model), BF),
            vm((n_sp, exp_dev, slots, dc), BF),
            vm((n_tp * fh, tok), BF),
            vm((exp_dev, n_tp * fh, n_rows), BF),
            vm((exp_dev, n_rows, dc), BF),
            vm((n_sp, exp_dev, slots, dc), BF),
            vm((experts * slots, tok), BF),
            vm((tok, experts * slots), BF),
            vm((experts, tok), F32),
            vm((exp_dev + 1, 2 * fh, d_model), BF),
            vm((exp_dev + 1, dc, n_tp * fh), BF),
            vm((tok, dc), BF),
            vm((tok, dc), F32),
            dma((2,)),
            dma((2,)),
            dma((4,)),
            dma((4,)),
            dma(()),
            dma((n_tp,)),
            dma(()),
            dma((n_chunk,)),
            dma(()),
            dma(()),
            dma(()),
            dma((n_tp,)),
            dma((n_chunk,)),
            dma((n_chunk, n_tp)),
            dma(()),
            dma((n_tp,)),
            dma((n_chunk,)),
            dma((n_chunk, n_tp)),
        ],
        compiler_params=pltpu.CompilerParams(
            collective_id=0, has_side_effects=True, vmem_limit_bytes=60 * 1024 * 1024
        ),
    )(
        queries,
        keys,
        values,
        sink.reshape(1, 1),
        w_out,
        stream,
        gain.reshape(1, d_model),
        routes.T,
        route_weights.T,
        w_gate,
        w_up,
        w_down,
        shared_gate,
        shared_up,
        shared_down,
    )


def solution(mesh, kv_group=4, order=Z_ORDER, nx=NX):
    placed = (
        P("sp", "tp"),
        P("sp", None),
        P("sp", None),
        P("tp"),
        P("tp", None),
        P(("sp", "tp"), None),
        P(),
        P("sp", None),
        P("sp", None),
        P("sp", "tp", None),
        P("sp", "tp", None),
        P("sp", None, "tp"),
        P("tp", None),
        P("tp", None),
        P(None, "tp"),
    )
    return jax.shard_map(
        functools.partial(local, kv_group=kv_group, order=order, nx=nx),
        mesh=mesh,
        in_specs=placed,
        out_specs=P("sp", "tp"),
        check_vma=False,
    )
```

time: 315 us -> 146 us (0.46)
  waiting for transfers between devices: 153 us -> 0 us
  Pallas kernels: 0 us -> 141 us
  blocking collectives: 58.3 us -> 0 us
  starting transfers between devices: 32.4 us -> 0 us
  local copies, waits for them, and re-layouts: 33.1 us -> 3.59 us
  matrix products: 17.8 us -> 0 us
  between operations: 14.5 us -> 0.68 us
  other arithmetic: 4.02 us -> 0 us
    pallas_call x0 -> x1, Pallas kernels: none -> 141 us  [local(): pl.pallas_call(functools.partial(kernel, kv_group=kv_group, order=order,...]
    all_gather x2 -> x0, waiting for transfers between devices: 93.2 us -> none  [the longest x1 49.5 us: local(): piece_rows = lax.all_gather(arrived, 'tp', axis=0, tiled=True)]
    all_to_all x5 -> x0, waiting for transfers between devices: 58.9 us -> none  [the longest x3 47.7 us: from_everyone(): return lax.all_to_all(copies, axis, split_axis=0, concat_axis=0, tiled=True)]
    all_to_all x2 -> x0, blocking collectives: 58.3 us -> none  [the longest x1 32 us: local(): lax.all_to_all(outgoing, 'sp', split_axis=0, concat_axis=0, tiled=True)]
    all_to_all x5 -> x0, starting transfers between devices: 29.2 us -> none  [the longest x3 10.7 us: from_everyone(): return lax.all_to_all(copies, axis, split_axis=0, concat_axis=0, tiled=True)]
    dot_general x11 -> x0, matrix products: 17.8 us -> none  [the longest x1 5.84 us: local(): jnp.einsum('tsecd,efd->tsecf', piece_rows, w_gate, preferred_element_type...]
    split x2 -> x0, local copies, waits for them, and re-layouts: 11.3 us -> none  [gather_turned(): jnp.split(result, [sum(widths[:k]) for k in range(1, len(widths))], axis=1)]
    reshape x3 -> x1, local copies, waits for them, and re-layouts: 7.41 us -> 0.6 us  [local(): gain.reshape(1, d_model)]
  transfers between devices with their start and end apart: 9 -> 0, of which waited for: 7 -> 0; matrix products, arithmetic and copies ran while one was open for 3% -> 0% of each run, Pallas kernels for 0% -> 0%
where the time goes in v1:
time: 146 us; the launch traced here: 145 us
  Pallas kernels  141 us (97%)
  local copies, waits for them, and re-layouts  3.59 us (2%)
    pallas_call x1, Pallas kernels, local(): pl.pallas_call(functools.partial(kernel, kv_group=kv_group, order=order,...  141 us
    unnamed x4, local copies, waits for them, and re-layouts  2.98 us

profile of v1, /device:TPU:1, one launch (start us, length us, event | category | flops | bytes accessed | tf_op | source)
XLA Modules:
  0.0 145.4 jit_solution(1896729229165578232)
XLA Ops:
  0.0 0.0 copy-start
  0.7 0.0 copy-done
  0.7 0.6 reshape.7.gain_ref
  1.3 1.5 %copy.16.q_ref = bf16[256,64]{1,0:T(8,128)(2,1)} copy(bf16[256,64]{0,1:T(8,128)(2,1)} %param.15) | data formatting | bytes 65536 | tf_op args[0]
  2.8 141.1 %shard_map.145 = bf16[256,128]{1,0:T(8,128)(2,1)} custom-call(bf16[256,64]{1,0:T(8,128)(2,1)} %copy.16.q_ref, bf16[256,256]{1,0:T(8,128)(2,1)} %k_ref.1, bf16[256,256]{1,0:T(8,128)(2,1)} %v_ref.1, f32[1,1]{1,0:T(1,128)} %bitcast.3.sink_ref, bf16[64,2048]{1,0:T(8,128)(2,1)} %w_out_ref.1, bf16[16,2048]{1,0:T(8,128)(2,1)} %stream_ref.1, ...), custom_call_target="tpu_custom_call" | custom-call | tf_op jit(solution)/shard_map/pallas_call | solution.py:562
  143.9 1.5 %copy.19 = bf16[256,128]{1,0:T(8,128)(2,1)} copy(bf16[256,128]{1,0:T(8,128)(2,1)} %shard_map.145) | data formatting | bytes 131072
Async XLA Ops:
  0.0 0.7 copy-start

commit v2 on v1

v2 whole, which is shorter than its diff:
```python
import collections
import contextlib
import functools

import jax
import jax.numpy as jnp
from jax import lax
from jax.experimental import pallas as pl
from jax.experimental.pallas import tpu as pltpu
from jax.sharding import PartitionSpec as P

HD = 64
WINDOW = 128
CAP = 2
NX = 4
NEAR = (0, 0, 1, 1, 1, 1, 1, 3)
DIRECT = 1
Z_ORDER = (1, 7, 2, 6, 3, 5, 4, 0)
NORM_EPS = 1e-05
mark = contextlib.nullcontext
BF = jnp.bfloat16
F32 = jnp.float32

NT = (((1,), (1,)), ((), ()))
TN = (((0,), (0,)), ((), ()))


def dot(a, b, dims=(((1,), (0,)), ((), ()))):
    return lax.dot_general(a, b, dims, preferred_element_type=F32)


def kernel(
    q_in,
    k_in,
    v_in,
    sink_in,
    w_out_in,
    stream_in,
    gain_in,
    routes_in,
    rw_in,
    w_gate_in,
    w_up_in,
    w_down_in,
    sg_in,
    su_in,
    sd_in,
    out_ref,
    q_ref,
    k_ref,
    v_ref,
    sink_ref,
    w_out_ref,
    stream_ref,
    gain_ref,
    routes_ref,
    rw_ref,
    w_gate_ref,
    w_up_ref,
    w_down_ref,
    sg_ref,
    su_ref,
    sd_ref,
    in_sem,
    wcol,
    scol,
    halo,
    abuf,
    sbuf,
    gbuf,
    obuf,
    hs,
    hbuf,
    ybuf,
    rbuf,
    ptab,
    ctab,
    stab,
    wexp,
    wdt,
    resid,
    shared_out,
    w_sem,
    wx_send,
    wx_recv,
    st_sem,
    halo_send,
    halo_recv,
    a_send,
    a_recv,
    d_send,
    d_recv,
    r_send,
    r_recv,
    ts_send,
    ts_recv,
    t_send,
    t_recv,
    hs_send,
    hs_recv,
    h_send,
    h_recv,
    *,
    kv_group,
    order,
    near,
    nx,
):
    hd, tok = q_ref.shape
    d_model = stream_ref.shape[1]
    rows_dev = stream_ref.shape[0]
    n_tp = lax.axis_size("tp")
    n_sp = lax.axis_size("sp")
    ny = n_tp // 2
    nz = n_sp // nx
    dc = d_model // n_tp
    exp_dev, fh = w_gate_ref.shape[0], w_gate_ref.shape[1]
    experts = exp_dev * n_sp
    topk = routes_ref.shape[0]
    slots = n_tp * CAP
    n_chunk = len(order)
    own_chunk = order.index(0)
    direct = [ny // 2 if k >= n_chunk - DIRECT else 0 for k in range(n_chunk)]
    crow = nx * slots
    sp = lax.axis_index("sp")
    tp = lax.axis_index("tp")
    y, c = tp // 2, tp % 2
    z, x = sp // nx, sp % nx
    half = ny // 2

    def cols(t):
        return pl.ds(pl.multiple_of(t * dc, dc), dc)

    def units(t):
        return pl.ds(pl.multiple_of(t * fh, fh), fh)

    def chip(dy):
        return lax.rem(y + dy + ny, ny)

    def remote(src, dst, send, recv, **device):
        return pltpu.make_async_remote_copy(
            src_ref=src,
            dst_ref=dst,
            send_sem=send,
            recv_sem=recv,
            device_id=device,
            device_id_type=pl.DeviceIdType.MESH,
        )

    def wait_for(ref, sem):
        pltpu.make_async_copy(ref, ref, sem).wait()

    pairs = (
        (q_in, q_ref),
        (k_in, k_ref),
        (v_in, v_ref),
        (sink_in, sink_ref),
        (w_out_in, w_out_ref),
        (stream_in, stream_ref),
        (gain_in, gain_ref),
        (routes_in, routes_ref),
        (rw_in, rw_ref),
        (w_gate_in, w_gate_ref),
        (w_up_in, w_up_ref),
        (w_down_in, w_down_ref),
        (sg_in, sg_ref),
        (su_in, su_ref),
        (sd_in, sd_ref),
    )

    def load(i):
        return pltpu.make_async_copy(pairs[i][0], pairs[i][1], in_sem.at[i])

    barrier = pltpu.get_barrier_semaphore()

    def greet_tp(i, carry):
        pl.semaphore_signal(barrier, inc=1, device_id={"tp": lax.rem(tp + i, n_tp)})
        return carry

    def greet_sp(i, carry):
        pl.semaphore_signal(barrier, inc=1, device_id={"sp": lax.rem(sp + i, n_sp)})
        return carry

    lax.fori_loop(1, n_tp, greet_tp, 0)
    lax.fori_loop(1, n_sp, greet_sp, 0)
    for i in (1, 2, 4, 5, 0, 3, 7, 8, 6, 9, 10, 12, 13, 11, 14):
        load(i).start()

    with mark("barrier"):
        pl.semaphore_wait(barrier, n_tp - 1 + n_sp - 1)

    head_kv = tp // kv_group
    pair = pl.ds(pl.multiple_of((head_kv // 2) * 2 * hd, 2 * hd), 2 * hd)
    last, first = sp == n_sp - 1, sp == 0
    to_next = lax.rem(sp + 1, n_sp)
    to_prev = lax.rem(sp + n_sp - 1, n_sp)

    def halo_copy(i):
        src = (k_ref, v_ref)[i % 2]
        rows = pl.ds(tok - WINDOW, WINDOW) if i < 2 else pl.ds(0, WINDOW)
        return remote(
            src.at[rows, pair],
            halo.at[i],
            halo_send.at[i],
            halo_recv.at[i],
            sp=to_next if i < 2 else to_prev,
        )

    share = w_out_ref.shape[0] // nx
    own_part = pl.ds(pl.multiple_of(x * share, share), share)

    def send_cols(i, carry):
        t = lax.rem(tp + i, n_tp)
        remote(
            w_out_ref.at[own_part, cols(t)], wcol.at[tp, own_part], w_sem.at[0], w_sem.at[1], tp=t
        ).start()
        return carry

    def send_stream(i, carry):
        t = lax.rem(tp + i, n_tp)
        remote(stream_ref.at[:, cols(t)], scol.at[tp], st_sem.at[0], st_sem.at[1], tp=t).start()
        return carry

    load(1).wait()
    load(2).wait()
    @pl.when(jnp.logical_not(last))
    def _():
        halo_copy(0).start()
        halo_copy(1).start()

    @pl.when(jnp.logical_not(first))
    def _():
        halo_copy(2).start()
        halo_copy(3).start()
    load(4).wait()
    lax.fori_loop(1, n_tp, send_cols, 0)
    load(5).wait()
    lax.fori_loop(1, n_tp, send_stream, 0)
    wcol[tp, own_part] = w_out_ref[own_part, cols(tp)]
    scol[tp] = stream_ref[:, cols(tp)]
    load(0).wait()
    load(3).wait()
    load(7).wait()
    load(8).wait()

    row_e = lax.broadcasted_iota(jnp.int32, (experts, tok), 0)
    hit_t = jnp.zeros((experts, tok), F32)
    weight_t = jnp.zeros((experts, tok), F32)
    for k in range(topk):
        hit = row_e == routes_ref[k : k + 1, :]
        hit_t = jnp.where(hit, 1.0, hit_t)
        weight_t = jnp.where(hit, rw_ref[k : k + 1, :], weight_t)
    early = lax.broadcasted_iota(jnp.int32, (tok, tok), 0)
    late = lax.broadcasted_iota(jnp.int32, (tok, tok), 1)
    before = (early < late) & (early // rows_dev == late // rows_dev)
    rank_t = dot(hit_t.astype(BF), jnp.where(before, 1.0, 0.0).astype(BF))
    slot_t = jnp.where(hit_t > 0, rank_t, -1.0)
    stab[...] = slot_t
    slot_row = lax.broadcasted_iota(jnp.int32, (slots, tok), 0)
    slot_tok = lax.broadcasted_iota(jnp.int32, (slots, tok), 1)
    in_block = (slot_row // CAP) == (slot_tok // rows_dev)
    slot_rank = jnp.where(in_block, slot_row % CAP, -2).astype(F32)

    def table_rows(e, carry):
        line = stab[pl.ds(e, 1), :]
        ptab[pl.ds(pl.multiple_of(e * slots, slots), slots), :] = jnp.where(
            line == slot_rank, 1.0, 0.0
        ).astype(BF)
        return carry

    lax.fori_loop(0, experts, table_rows, 0)

    @pl.when(first)
    def _():
        halo[0] = jnp.zeros(halo.shape[1:], BF)
        halo[1] = jnp.zeros(halo.shape[1:], BF)

    @pl.when(last)
    def _():
        halo[2] = jnp.zeros(halo.shape[1:], BF)
        halo[3] = jnp.zeros(halo.shape[1:], BF)

    with mark("halo_wait"):
        @pl.when(jnp.logical_not(first))
        def _():
            halo_copy(0).wait_recv()
            halo_copy(1).wait_recv()

        @pl.when(jnp.logical_not(last))
        def _():
            halo_copy(2).wait_recv()
            halo_copy(3).wait_recv()

    odd = head_kv % 2
    query = q_ref[...]
    empty = jnp.zeros_like(query)
    query = jnp.concatenate(
        [jnp.where(odd == 0, query, empty), jnp.where(odd == 0, empty, query)], axis=0
    )
    sink = sink_ref[0:1, 0:1]
    key_i = lax.broadcasted_iota(jnp.int32, (WINDOW, WINDOW), 0)
    query_i = lax.broadcasted_iota(jnp.int32, (WINDOW, WINDOW), 1)
    blocks = tok // WINDOW
    for n in range(blocks):
        q_n = query[:, n * WINDOW : (n + 1) * WINDOW]
        parts = []
        for j in (-1, 0, 1):
            b = n + j
            if b < 0:
                key, value = halo[0], halo[1]
                allowed = (query_i <= key_i) & jnp.logical_not(first)
            elif b == blocks:
                key, value = halo[2], halo[3]
                allowed = (key_i <= query_i) & jnp.logical_not(last)
            else:
                rows = pl.ds(b * WINDOW, WINDOW)
                key, value = k_ref[rows, pair], v_ref[rows, pair]
                allowed = (query_i <= key_i, None, key_i <= query_i)[j + 1]
            score = dot(key, q_n) * (hd**-0.5)
            if allowed is not None:
                score = jnp.where(allowed, score, -jnp.inf)
            parts.append((score, value))
        peak = jnp.maximum(sink, jnp.max(parts[0][0], axis=0, keepdims=True))
        for score, _v in parts[1:]:
            peak = jnp.maximum(peak, jnp.max(score, axis=0, keepdims=True))
        exps = [jnp.exp(score - peak) for score, _v in parts]
        total = jnp.exp(sink - peak)
        for e in exps:
            total = total + jnp.sum(e, axis=0, keepdims=True)
        mix = None
        for e, (_s, value) in zip(exps, parts):
            prob = (e / total).astype(BF)
            term = dot(value, prob, TN)
            mix = term if mix is None else mix + term
        mine = jnp.where(odd == 0, mix[:hd], mix[hd:])
        abuf[tp, :, n * WINDOW : (n + 1) * WINDOW] = mine.astype(BF)

    def peer_of(t):
        return 2 * (t // 2) + 1 - t % 2

    partner = peer_of(tp)

    def to_partner(t):
        return remote(abuf.at[t], abuf.at[t], a_send, a_recv.at[t], tp=partner)

    def to_chip(t, h):
        return remote(abuf.at[t], abuf.at[t], a_send, a_recv.at[t], tp=2 * chip(h) + c)

    for h in range(half, 0, -1):
        to_chip(tp, h).start()
        if h < half:
            to_chip(tp, -h).start()
    to_partner(tp).start()

    def w_along_x(j):
        part = wcol.at[:, own_part]
        to = z * nx + lax.rem(x + j, nx)
        return remote(part, part, wx_send.at[j - 1], wx_recv.at[j - 1], sp=to)

    with mark("w_wait"):
        wait_for(wcol.at[pl.ds(0, n_tp - 1), own_part], w_sem.at[1])
    for j in range(1, nx):
        w_along_x(j).start()

    for i in (6, 9, 10, 12, 13, 11, 14):
        load(i).wait()
    for i in range(d_model // 128):
        some = slice(i * 128, (i + 1) * 128)
        gain = gain_ref[i : i + 1, :].astype(F32)
        for e in range(exp_dev):
            wexp[e, :fh, some] = (w_gate_ref[e, :, some].astype(F32) * gain).astype(BF)
            wexp[e, fh:, some] = (w_up_ref[e, :, some].astype(F32) * gain).astype(BF)
        wexp[exp_dev, :fh, some] = (sg_ref[:, some].astype(F32) * gain).astype(BF)
        wexp[exp_dev, fh:, some] = (su_ref[:, some].astype(F32) * gain).astype(BF)

    with mark("att_wait"):
        for h in range(1, half + 1):
            for sign in (1, -1):
                if h == half and sign == -1:
                    continue
                t = 2 * chip(-sign * h) + c
                wait_for(abuf.at[t], a_recv.at[t])
                to_partner(t).start()

    for e in range(exp_dev):
        wdt[e] = w_down_ref[e].astype(F32).T.astype(BF)
    wdt[exp_dev] = sd_ref[...].astype(F32).T.astype(BF)

    with mark("att_wait2"):
        for j in range(1, nx):
            w_along_x(j).wait_recv()
        wait_for(scol.at[pl.ds(0, n_tp - 1)], st_sem.at[1])
        for i in range(ny):
            t = 2 * chip(i) + 1 - c
            wait_for(abuf.at[t], a_recv.at[t])
    projected = dot(
        abuf[...].reshape(n_tp * hd, tok), wcol[...].reshape(n_tp * hd, dc), TN
    )
    mixed = (scol[...].reshape(tok, dc).astype(F32) + projected).astype(BF)
    resid[...] = mixed
    sbuf[:, cols(tp)] = mixed

    def dest(i, j):
        return lax.rem(z - order[i] + nz, nz) * nx + lax.rem(x + j, nx)

    def source(i, j):
        return lax.rem(z + order[i], nz) * nx + lax.rem(x + j, nx)

    def spot(pos):
        return pl.ds(pl.multiple_of(pos * slots, slots), slots)

    def chunk_rows(k):
        return pl.ds(pl.multiple_of(k * crow, crow), crow)

    def ring_start(block, send, recv, near=0):
        for t in (2 * chip(1) + c, 2 * chip(-1) + c, partner)[2 if near else 0 :]:
            remote(block(tp), block(tp), send, recv(tp), tp=t).start()

    def pass_on(block, send, recv, h, sign, near=0):
        t = 2 * chip(-sign * h) + c
        onto = 2 * chip(sign) + c
        if near <= h < half - 1:
            remote(block(t), block(t), send, recv(t), tp=onto).start()
        elif near <= h == half - 1:

            @pl.when(c == (0 if sign == 1 else 1))
            def _():
                remote(block(t), block(t), send, recv(t), tp=onto).start()

        remote(block(t), block(t), send, recv(t), tp=partner).start()

    def ring_hop(block, send, recv, h, near=0):
        for sign in (1, -1):
            if h < half or sign == 1:
                t = 2 * chip(-sign * h) + c
                wait_for(block(t), recv(t))
                pass_on(block, send, recv, h, sign, near)

    def to_all(block, send, recv):
        for h in range(half, 0, -1):
            for sign in (1, -1):
                if h < half or sign == 1:
                    onto = 2 * chip(sign * h) + c
                    remote(block(tp), block(tp), send, recv(tp), tp=onto).start()
        remote(block(tp), block(tp), send, recv(tp), tp=partner).start()

    def ring_end(block, recv):
        for i in range(ny):
            t = 2 * chip(i) + 1 - c
            wait_for(block(t), recv(t))

    tok_shared = (
        lambda t: sbuf.at[:, cols(t)],
        ts_send,
        lambda t: ts_recv.at[t],
    )
    hid_shared = (
        lambda t: hs.at[units(t), :],
        hs_send,
        lambda t: hs_recv.at[t],
    )

    def tok_ring(k):
        return (
            lambda t: gbuf.at[:, chunk_rows(k), cols(t)],
            t_send.at[k],
            lambda t: t_recv.at[k, t],
        )

    def hid_ring(k):
        return (
            lambda t: hbuf.at[:, units(t), chunk_rows(k)],
            h_send.at[k],
            lambda t: h_recv.at[k, t],
        )

    ring_start(*tok_shared)
    pieces = min(4, n_sp)
    count = n_sp // pieces
    with mark("dispdot"):
        for part in range(pieces):
            size = count * exp_dev * slots
            rows = dot(ptab[part * size : (part + 1) * size, :], mixed)
            obuf[part * count : (part + 1) * count] = rows.astype(BF).reshape(
                count, exp_dev, slots, dc
            )

    def shown(n):
        return 2 * chip((n + 1) // 2 * (-1 if n % 2 else 1)) + c

    def send_rows(n, i):
        for j in range(nx):
            if i == own_chunk and j == 0:
                gbuf[:, spot(i * nx + x), cols(shown(n))] = obuf[n * n_sp + sp]
            else:
                d = dest(i, j)
                remote(
                    obuf.at[n * n_sp + d],
                    gbuf.at[:, spot(i * nx + x), cols(shown(n))],
                    d_send,
                    d_recv.at[i, n],
                    sp=d,
                ).start()

    def beside(h):
        return jnp.concatenate(
            [sbuf[:, cols(shown(2 * h - 1))], sbuf[:, cols(shown(2 * h))]], axis=1
        )

    def make_rows(h, at, blocks, both):
        size = exp_dev * slots
        some = pl.ds(pl.multiple_of(at * size, size), blocks * size)
        rows = dot(ptab[some, :], both)
        for n in (2 * h - 1, 2 * h):
            half_rows = rows[:, :dc] if n % 2 else rows[:, dc:]
            obuf[pl.ds(n * n_sp + at, blocks)] = half_rows.astype(BF).reshape(
                blocks, exp_dev, slots, dc
            )

    def rows_arrived(n, k):
        rows = (nx - (1 if k == own_chunk else 0)) * slots
        if rows:
            wait_for(gbuf.at[:, pl.ds(0, rows), cols(tp)], d_recv.at[k, n])

    def inject(h):
        both = beside(h)
        takers = [i for i in range(n_chunk) if near[i] >= h]
        if 2 * len(takers) > n_chunk:
            for part in range(pieces):
                make_rows(h, part * count, count, both)
        else:
            for i in takers:
                make_rows(h, lax.rem(z - order[i] + nz, nz) * nx, nx, both)
        for i in range(n_chunk):
            if h == 1 and i >= ahead:
                send_rows(0, i)
            if near[i] >= h:
                send_rows(2 * h - 1, i)
                send_rows(2 * h, i)

    ahead = min(4, n_chunk)
    for i in range(ahead):
        send_rows(0, i)

    slot_c = slot_t.T.astype(BF)
    weight_c = weight_t.T.astype(BF)
    width = min(512, experts * slots)
    for part in range(experts * slots // width):
        m = lax.broadcasted_iota(jnp.int32, (experts, width), 1) + part * width
        e_i = lax.broadcasted_iota(jnp.int32, (experts, width), 0)
        spread = jnp.where(m // slots == e_i, 1.0, 0.0).astype(BF)
        m2 = lax.broadcasted_iota(jnp.int32, (tok, width), 1) + part * width
        r2 = lax.broadcasted_iota(jnp.int32, (tok, width), 0)
        want = jnp.where((m2 % slots) // CAP == r2 // rows_dev, m2 % CAP, -2).astype(F32)
        table = jnp.where(dot(slot_c, spread) == want, dot(weight_c, spread), 0.0)
        ctab[:, part * width : (part + 1) * width] = table.astype(BF)

    def hidden_of(rows, e):
        wide = rows.astype(F32)
        squares = wide * wide
        part = squares[:, :128]
        for i in range(1, d_model // 128):
            part = part + squares[:, i * 128 : (i + 1) * 128]
        total = jnp.sum(part.T, axis=0, keepdims=True)
        scale = lax.rsqrt(total / d_model + NORM_EPS)
        acts = dot(wexp[e], rows, NT) * scale
        gate, up = acts[:fh], acts[fh:]
        return (gate / (1.0 + jnp.exp(-gate)) * up).astype(BF)

    def up_shared():
        ring_end(tok_shared[0], tok_shared[2])
        hs[units(tp), :] = hidden_of(sbuf[...], exp_dev)
        ring_start(*hid_shared)

    def up_chunk(k):
        ring_end(tok_ring(k)[0], tok_ring(k)[2])
        for e in range(exp_dev):
            hbuf[e, units(tp), chunk_rows(k)] = hidden_of(gbuf[e, chunk_rows(k), :], e)
        if direct[k]:
            to_all(*hid_ring(k))
        else:
            ring_start(*hid_ring(k))

    def down_shared():
        ring_end(hid_shared[0], hid_shared[2])
        shared_out[...] = dot(wdt[exp_dev], hs[...]).T

    def down_chunk(k):
        ring_end(hid_ring(k)[0], hid_ring(k)[2])
        for e in range(exp_dev):
            res = dot(wdt[e], hbuf[e, :, chunk_rows(k)])
            ybuf[e, chunk_rows(k), :] = res.T.astype(BF)
        return_chunk(k)

    def give_back(i, j):
        s = source(i, j)
        pos = i * nx + lax.rem(x + j, nx)
        return remote(ybuf.at[:, spot(pos), :], rbuf.at[sp], r_send, r_recv, sp=s)

    def return_chunk(k):
        for j in range(nx):
            if k == own_chunk and j == 0:
                rbuf[sp] = ybuf[:, spot(k * nx + x), :]
            else:
                give_back(k, j).start()

    def tok_in(k):
        rows_arrived(0, k)
        ring_start(*tok_ring(k), near[k])
        for h in range(1, near[k] + 1):
            for n, sign in ((2 * h - 1, 1), (2 * h, -1)):
                rows_arrived(n, k)
                pass_on(*tok_ring(k), h, sign, near[k])

    slots_of = collections.defaultdict(list)
    for h in range(1, half + 1):
        slots_of[h - 2].append((2, f"tokS_{h}", lambda h=h: ring_hop(*tok_shared, h)))
        slots_of[half - 2 + h].append((1, f"hidS_{h}", lambda h=h: ring_hop(*hid_shared, h)))
    slots_of[half - 2].append((3, "upS", up_shared))
    slots_of[2 * half - 2].append((4, "downS", down_shared))
    for h in range(1, max(half, 2)):
        slots_of[h - 2].append((3, f"inject{h}", lambda h=h: inject(h)))
    for k in range(n_chunk):
        up_at = k + half - 1
        slots_of[up_at - half + near[k]].append((2, f"in{k}", lambda k=k: tok_in(k)))
        for h in range(near[k] + 1, half + 1):
            slots_of[up_at - half + h].append(
                (2, f"tok{k}_{h}", lambda k=k, h=h: ring_hop(*tok_ring(k), h))
            )
        slots_of[up_at].append((3, f"up{k}", lambda k=k: up_chunk(k)))
        for h in range(1, half + 1):
            slots_of[up_at + (half if direct[k] else h)].append(
                (1, f"hid{k}_{h}", lambda k=k, h=h: ring_hop(*hid_ring(k), h, direct[k]))
            )
        slots_of[up_at + half].append((4, f"down{k}", lambda k=k: down_chunk(k)))
    for slot in sorted(slots_of):
        for _r, name, step in sorted(slots_of[slot], key=lambda item: item[0]):
            with mark(name):
                step()

    wait_for(wcol.at[pl.ds(0, n_tp - 1), own_part], w_sem.at[0])
    for j in range(1, nx):
        w_along_x(j).wait_send()
    wait_for(scol.at[pl.ds(0, n_tp - 1)], st_sem.at[0])

    @pl.when(jnp.logical_not(last))
    def _():
        halo_copy(0).wait_send()
        halo_copy(1).wait_send()

    @pl.when(jnp.logical_not(first))
    def _():
        halo_copy(2).wait_send()
        halo_copy(3).wait_send()

    wait_for(abuf.at[pl.ds(0, n_tp - 1)], a_send)
    count = sum((1 + 2 * near[i]) * (nx - (i == own_chunk)) for i in range(n_chunk))
    wait_for(obuf.at[pl.ds(0, count)], d_send)
    wait_for(sbuf.at[:, pl.ds(0, (n_tp - 1) * dc)], ts_send)
    wait_for(hs.at[pl.ds(0, (n_tp - 1) * fh), :], hs_send)
    for k in range(n_chunk):
        wait_for(
            gbuf.at[:, chunk_rows(k), pl.ds(0, (n_tp - 1 - 2 * near[k]) * dc)], t_send.at[k]
        )
        wait_for(hbuf.at[:, pl.ds(0, (n_tp - 1) * fh), chunk_rows(k)], h_send.at[k])
    wait_for(rbuf.at[pl.ds(0, n_sp - 1)], r_send)

    with mark("ret_wait"):
        wait_for(rbuf.at[pl.ds(0, n_sp - 1)], r_recv)
    with mark("combine"):
        routed = dot(ctab[...], rbuf[...].reshape(experts * slots, dc))
        out_ref[...] = (resid[...].astype(F32) + routed + shared_out[...]).astype(BF)


def local(
    queries,
    keys,
    values,
    sink,
    w_out,
    stream,
    gain,
    routes,
    route_weights,
    w_gate,
    w_up,
    w_down,
    shared_gate,
    shared_up,
    shared_down,
    *,
    kv_group,
    order,
    near,
    nx,
):
    n_tp = lax.axis_size("tp")
    n_sp = lax.axis_size("sp")
    tok = queries.shape[0]
    rows, d_model = stream.shape
    dc = d_model // n_tp
    exp_dev, fh, _ = w_gate.shape
    experts = exp_dev * n_sp
    slots = n_tp * CAP
    n_rows = n_sp * slots
    n_chunk = len(order)
    vm = pltpu.VMEM
    dma = pltpu.SemaphoreType.DMA
    inputs = (
        queries.T,
        keys,
        values,
        sink.reshape(1, 1),
        w_out,
        stream,
        gain.reshape(d_model // 128, 128),
        routes.T,
        route_weights.T,
        w_gate,
        w_up,
        w_down,
        shared_gate,
        shared_up,
        shared_down,
    )
    return pl.pallas_call(
        functools.partial(kernel, kv_group=kv_group, order=order, near=near, nx=nx),
        out_shape=jax.ShapeDtypeStruct((tok, dc), BF),
        in_specs=[pl.BlockSpec(memory_space=pl.ANY)] * 15,
        out_specs=pl.BlockSpec(memory_space=vm),
        scratch_shapes=[
            *[vm(a.shape, a.dtype) for a in inputs],
            dma((len(inputs),)),
            vm((n_tp, w_out.shape[0], dc), BF),
            vm((n_tp, rows, dc), BF),
            vm((4, WINDOW, 2 * HD), BF),
            vm((n_tp, HD, tok), BF),
            vm((tok, d_model), BF),
            vm((exp_dev, n_rows, d_model), BF),
            vm(((1 + 2 * max(near)) * n_sp, exp_dev, slots, dc), BF),
            vm((n_tp * fh, tok), BF),
            vm((exp_dev, n_tp * fh, n_rows), BF),
            vm((exp_dev, n_rows, dc), BF),
            vm((n_sp, exp_dev, slots, dc), BF),
            vm((experts * slots, tok), BF),
            vm((tok, experts * slots), BF),
            vm((experts, tok), F32),
            vm((exp_dev + 1, 2 * fh, d_model), BF),
            vm((exp_dev + 1, dc, n_tp * fh), BF),
            vm((tok, dc), BF),
            vm((tok, dc), F32),
            dma((2,)),
            dma((max(nx - 1, 1),)),
            dma((max(nx - 1, 1),)),
            dma((2,)),
            dma((4,)),
            dma((4,)),
            dma(()),
            dma((n_tp,)),
            dma(()),
            dma((n_chunk, 1 + 2 * max(near))),
            dma(()),
            dma(()),
            dma(()),
            dma((n_tp,)),
            dma((n_chunk,)),
            dma((n_chunk, n_tp)),
            dma(()),
            dma((n_tp,)),
            dma((n_chunk,)),
            dma((n_chunk, n_tp)),
        ],
        compiler_params=pltpu.CompilerParams(
            collective_id=0, has_side_effects=True, vmem_limit_bytes=60 * 1024 * 1024
        ),
    )(*inputs)


def solution(mesh, kv_group=4, order=Z_ORDER, near=NEAR, nx=NX):
    placed = (
        P("sp", "tp"),
        P("sp", None),
        P("sp", None),
        P("tp"),
        P("tp", None),
        P(("sp", "tp"), None),
        P(),
        P("sp", None),
        P("sp", None),
        P("sp", "tp", None),
        P("sp", "tp", None),
        P("sp", None, "tp"),
        P("tp", None),
        P("tp", None),
        P(None, "tp"),
    )
    return jax.shard_map(
        functools.partial(local, kv_group=kv_group, order=order, near=near, nx=nx),
        mesh=mesh,
        in_specs=placed,
        out_specs=P("sp", "tp"),
        check_vma=False,
    )
```

time: 146 us -> 125 us (0.86)
  Pallas kernels: 141 us -> 123 us
  local copies, waits for them, and re-layouts: 3.59 us -> 1.47 us
    pallas_call x1, Pallas kernels: 141 us -> 123 us  [local(): pl.pallas_call(functools.partial(kernel, kv_group=kv_group, order=order,...]
    unnamed x4 -> x1, local copies, waits for them, and re-layouts: 2.98 us -> 1.47 us
where the time goes in v2:
time: 125 us
  Pallas kernels  123 us (98%)
  local copies, waits for them, and re-layouts  1.47 us (1%)
    pallas_call x1, Pallas kernels, local(): pl.pallas_call(functools.partial(kernel, kv_group=kv_group, order=order,...  123 us

profile of v2, /device:TPU:1, one launch (start us, length us, event | category | flops | bytes accessed | tf_op | source)
XLA Modules:
  0.0 125.1 jit_solution(9802540365546598742)
XLA Ops:
  0.7 122.9 %shard_map.145 = bf16[256,128]{1,0:T(8,128)(2,1)} custom-call(bf16[64,256]{1,0:T(8,128)(2,1)} %bitcast.6, bf16[256,256]{1,0:T(8,128)(2,1)} %k_in.1, bf16[256,256]{1,0:T(8,128)(2,1)} %v_in.1, f32[1,1]{1,0:T(1,128)} %bitcast.5.sink_in, bf16[64,2048]{1,0:T(8,128)(2,1)} %w_out_in.1, bf16[16,2048]{1,0:T(8,128)(2,1)} %stream_in.1, bf16[16,128]{1,0:T(8,128)(2,1)} %bitcast.7, ...), custom_call_target="tpu_custom_call" | custom-call | tf_op jit(solution)/shard_map/pallas_call | solution.py:726
  123.6 1.5 %copy.18 = bf16[256,128]{1,0:T(8,128)(2,1)} copy(bf16[256,128]{1,0:T(8,128)(2,1)} %shard_map.145) | data formatting | bytes 131072

commit v3 on v2

--- a/solution.py
+++ b/solution.py
@@ -13,9 +13,9 @@
 WINDOW = 128
 CAP = 2
 NX = 4
-NEAR = (0, 0, 1, 1, 1, 1, 1, 3)
-DIRECT = 1
-Z_ORDER = (1, 7, 2, 6, 3, 5, 4, 0)
+NEAR = (0, 0, 0, 1, 1, 1, 3, 3)
+DIRECT = 0
+Z_ORDER = (1, 2, 3, 6, 5, 4, 7, 0)
 NORM_EPS = 1e-05
 mark = contextlib.nullcontext
 BF = jnp.bfloat16
@@ -576,9 +576,7 @@
         ring_end(tok_ring(k)[0], tok_ring(k)[2])
         for e in range(exp_dev):
             hbuf[e, units(tp), chunk_rows(k)] = hidden_of(gbuf[e, chunk_rows(k), :], e)
-        if direct[k]:
-            to_all(*hid_ring(k))
-        else:
+        if not direct[k]:
             ring_start(*hid_ring(k))
 
     def down_shared():
@@ -621,13 +619,16 @@
     for h in range(1, max(half, 2)):
         slots_of[h - 2].append((3, f"inject{h}", lambda h=h: inject(h)))
     for k in range(n_chunk):
-        up_at = k + half - 1
-        slots_of[up_at - half + near[k]].append((2, f"in{k}", lambda k=k: tok_in(k)))
+        full_at = k + half - 1 - (k == n_chunk - 1)
+        slots_of[full_at - half + near[k]].append((2, f"in{k}", lambda k=k: tok_in(k)))
         for h in range(near[k] + 1, half + 1):
-            slots_of[up_at - half + h].append(
+            slots_of[full_at - half + h].append(
                 (2, f"tok{k}_{h}", lambda k=k, h=h: ring_hop(*tok_ring(k), h))
             )
-        slots_of[up_at].append((3, f"up{k}", lambda k=k: up_chunk(k)))
+        up_at = full_at + 1
+        slots_of[up_at].append((1.5, f"up{k}", lambda k=k: up_chunk(k)))
+        if direct[k]:
+            slots_of[up_at + 1].append((1.5, f"hid{k}", lambda k=k: to_all(*hid_ring(k))))
         for h in range(1, half + 1):
             slots_of[up_at + (half if direct[k] else h)].append(
                 (1, f"hid{k}_{h}", lambda k=k, h=h: ring_hop(*hid_ring(k), h, direct[k]))

time: 125 us -> 119 us (0.952)
  Pallas kernels: 123 us -> 117 us
    pallas_call x1, Pallas kernels: 123 us -> 117 us  [local(): pl.pallas_call(functools.partial(kernel, kv_group=kv_group, order=order,...]
where the time goes in v3:
time: 119 us
  Pallas kernels  117 us (98%)
  local copies, waits for them, and re-layouts  1.47 us (1%)
    pallas_call x1, Pallas kernels, local(): pl.pallas_call(functools.partial(kernel, kv_group=kv_group, order=order,...  117 us

profile of v3, /device:TPU:1, one launch (start us, length us, event | category | flops | bytes accessed | tf_op | source)
XLA Modules:
  0.0 118.9 jit_solution(6673720417922571806)
XLA Ops:
  0.7 116.8 %shard_map.145 = bf16[256,128]{1,0:T(8,128)(2,1)} custom-call(bf16[64,256]{1,0:T(8,128)(2,1)} %bitcast.6, bf16[256,256]{1,0:T(8,128)(2,1)} %k_in.1, bf16[256,256]{1,0:T(8,128)(2,1)} %v_in.1, f32[1,1]{1,0:T(1,128)} %bitcast.5.sink_in, bf16[64,2048]{1,0:T(8,128)(2,1)} %w_out_in.1, bf16[16,2048]{1,0:T(8,128)(2,1)} %stream_in.1, bf16[16,128]{1,0:T(8,128)(2,1)} %bitcast.7, ...), custom_call_target="tpu_custom_call" | custom-call | tf_op jit(solution)/shard_map/pallas_call | solution.py:727
  117.4 1.5 %copy.18 = bf16[256,128]{1,0:T(8,128)(2,1)} copy(bf16[256,128]{1,0:T(8,128)(2,1)} %shard_map.145) | data formatting | bytes 131072

commit v4 on v3

--- a/solution.py
+++ b/solution.py
@@ -13,9 +13,10 @@
 WINDOW = 128
 CAP = 2
 NX = 4
-NEAR = (0, 0, 0, 1, 1, 1, 3, 3)
+NEAR = (0, 0, 0, 0, 3, 1, 3, 3)
+FULL = (3, 4, 5, 6, 6, 7, 7, 8)
 DIRECT = 0
-Z_ORDER = (1, 2, 3, 6, 5, 4, 7, 0)
+Z_ORDER = (1, 6, 3, 4, 0, 5, 2, 7)
 NORM_EPS = 1e-05
 mark = contextlib.nullcontext
 BF = jnp.bfloat16
@@ -538,7 +539,7 @@
                 send_rows(2 * h - 1, i)
                 send_rows(2 * h, i)
 
-    ahead = min(4, n_chunk)
+    ahead = min(5, n_chunk)
     for i in range(ahead):
         send_rows(0, i)
 
@@ -613,13 +614,13 @@
     slots_of = collections.defaultdict(list)
     for h in range(1, half + 1):
         slots_of[h - 2].append((2, f"tokS_{h}", lambda h=h: ring_hop(*tok_shared, h)))
-        slots_of[half - 2 + h].append((1, f"hidS_{h}", lambda h=h: ring_hop(*hid_shared, h)))
-    slots_of[half - 2].append((3, "upS", up_shared))
-    slots_of[2 * half - 2].append((4, "downS", down_shared))
+        slots_of[half - 1 + h].append((2.9, f"hidS_{h}", lambda h=h: ring_hop(*hid_shared, h)))
+    slots_of[half - 1].append((1.5, "upS", up_shared))
+    slots_of[2 * half + 1].append((1.6, "downS", down_shared))
     for h in range(1, max(half, 2)):
-        slots_of[h - 2].append((3, f"inject{h}", lambda h=h: inject(h)))
+        slots_of[h - 2].append((2 if h == 1 else 3, f"inject{h}", lambda h=h: inject(h)))
     for k in range(n_chunk):
-        full_at = k + half - 1 - (k == n_chunk - 1)
+        full_at = FULL[k] + half - 4
         slots_of[full_at - half + near[k]].append((2, f"in{k}", lambda k=k: tok_in(k)))
         for h in range(near[k] + 1, half + 1):
             slots_of[full_at - half + h].append(

time: 119 us -> 113 us (0.950)
  Pallas kernels: 117 us -> 111 us
    pallas_call x1, Pallas kernels: 117 us -> 111 us  [local(): pl.pallas_call(functools.partial(kernel, kv_group=kv_group, order=order,...]
where the time goes in v4:
time: 113 us
  Pallas kernels  111 us (98%)
  local copies, waits for them, and re-layouts  1.47 us (1%)
    pallas_call x1, Pallas kernels, local(): pl.pallas_call(functools.partial(kernel, kv_group=kv_group, order=order,...  111 us

profile of v4, /device:TPU:1, one launch (start us, length us, event | category | flops | bytes accessed | tf_op | source)
XLA Modules:
  0.0 113.1 jit_solution(3213997816809902937)
XLA Ops:
  0.7 110.9 %shard_map.145 = bf16[256,128]{1,0:T(8,128)(2,1)} custom-call(bf16[64,256]{1,0:T(8,128)(2,1)} %bitcast.6, bf16[256,256]{1,0:T(8,128)(2,1)} %k_in.1, bf16[256,256]{1,0:T(8,128)(2,1)} %v_in.1, f32[1,1]{1,0:T(1,128)} %bitcast.5.sink_in, bf16[64,2048]{1,0:T(8,128)(2,1)} %w_out_in.1, bf16[16,2048]{1,0:T(8,128)(2,1)} %stream_in.1, bf16[16,128]{1,0:T(8,128)(2,1)} %bitcast.7, ...), custom_call_target="tpu_custom_call" | custom-call | tf_op jit(solution)/shard_map/pallas_call | solution.py:728
  111.6 1.5 %copy.18 = bf16[256,128]{1,0:T(8,128)(2,1)} copy(bf16[256,128]{1,0:T(8,128)(2,1)} %shard_map.145) | data formatting | bytes 131072
